TPU v7x, 512 devices: a 8x2x16 block of a 8x8x16 slice. The times are simulated.
512 devices in a mesh: grp: 2 (over y), sp: 16 (over z), dp: 16 (over x, core).
Axes of the slice: x: 8, y: 2, z: 16, core: 2. Of those that a mesh axis runs over, the one named last changes fastest.
The devices are a block of a 8x8x16 slice.
Arguments:
- queries: bfloat16 [32, 2048, 16, 192], P(('grp', 'dp'), 'sp'), parts along dimension 0, may hold values from -41 to 41
- kv_latent: bfloat16 [32, 2048, 512], P(('grp', 'dp'), 'sp'), parts along dimension 0, may hold values from -6 to 6
- rope_key: bfloat16 [32, 2048, 64], P(('grp', 'dp'), 'sp'), parts along dimension 0, may hold values from -5.1 to 5.1
- kv_gain: float32 [512], replicated, may hold values from 0.1 to 1.9
- kv_weight: bfloat16 [512, 4096], P('dp', 'sp'), may hold values from -0.25 to 0.25
- out_weight: bfloat16 [2048, 2048], P(None, 'dp'), may hold values from -1 to 1
Outputs:
- mixed: bfloat16 [32, 2048, 2048], P(('grp', 'dp'), 'sp'), parts along dimension 0
There are 2 independent parts, one for each index of `grp`. A program takes and returns all parts, laid end to end along the dimension named above; an argument that names none is the same for every part. Nothing has to cross between parts.
All inputs are finite; a program needn't handle non-finite values.
Results may differ from a plain program's by a relative error of at most 0.0075.
Values may be sent and summed in bfloat16 or wider, within the bound.
A program may use at most 64 MiB of HBM per device.

v0:
```python
import jax
import jax.numpy as jnp
from jax import lax
from jax.sharding import PartitionSpec as P

NOPE = 128
VD = 128


def sent_to_all(value, axis):
    length = lax.axis_size(axis)
    return lax.all_to_all(
        jnp.broadcast_to(value[None], (length, *value.shape)), axis, 0, 0, tiled=True
    )


def in_order(parts, dim):
    parts = jnp.moveaxis(parts, 0, dim)
    dims = parts.shape
    return parts.reshape(*dims[:dim], dims[dim] * dims[dim + 1], *dims[dim + 2 :])


def gather_directly(value, axis, dim):
    parts = sent_to_all(value, axis)
    return in_order(parts, dim)


def rotate(values, positions):
    half = values.shape[-1] // 2
    inverse = jnp.power(10000.0, -jnp.arange(half, dtype=jnp.float32) * 2.0 / values.shape[-1])
    angle = positions.astype(jnp.float32)[..., None] * inverse
    first = values[..., :half].astype(jnp.float32)
    second = values[..., half:].astype(jnp.float32)
    cosine = jnp.cos(angle)
    sine = jnp.sin(angle)
    return jnp.concatenate(
        [first * cosine - second * sine, first * sine + second * cosine], axis=-1
    )


def attend(query_rot, key_value, key_rot):
    length, heads = (query_rot.shape[0], query_rot.shape[1])
    nope = query_rot.shape[2] - key_rot.shape[1]
    scale = query_rot.shape[2] ** (-0.5)
    content = key_value[:, :, :nope]
    values = key_value[:, :, nope:]
    shared = key_rot[:, None, :]
    keys = jnp.concatenate([content, shared], axis=-1)
    block = min(512, length)
    blocks = query_rot.reshape(length // block, block, heads, query_rot.shape[2])
    key_pos = jnp.arange(length, dtype=jnp.int32)

    def one_block(item):
        query_block, index = item
        scores = (
            jnp.einsum("qhd,khd->hqk", query_block, keys, preferred_element_type=jnp.float32)
            * scale
        )
        query_pos = index * block + jnp.arange(block, dtype=jnp.int32)
        kept = query_pos[:, None] >= key_pos[None, :]
        scores = jnp.where(kept[None], scores, -jnp.inf)
        top = jnp.max(scores, axis=-1, keepdims=True)
        expo = jnp.exp(scores - top)
        probs = (expo / jnp.sum(expo, axis=-1, keepdims=True)).astype(jnp.bfloat16)
        return jnp.einsum("hqk,khd->qhd", probs, values, preferred_element_type=jnp.float32).astype(
            jnp.bfloat16
        )

    result = lax.map(one_block, (blocks, jnp.arange(length // block, dtype=jnp.int32)))
    return result.reshape(length, heads, values.shape[2])


def body(queries, kv_latent, rope_key, kv_gain, kv_weight, out_weight):
    tok_rows = queries.shape[1]
    positions = lax.axis_index("sp") * tok_rows + jnp.arange(tok_rows, dtype=jnp.int32)
    latent32 = kv_latent[0].astype(jnp.float32)
    latent_n = (
        latent32
        * lax.rsqrt(jnp.mean(latent32 * latent32, axis=-1, keepdims=True) + 1e-06)
        * kv_gain
    ).astype(jnp.bfloat16)
    key_rot = rotate(rope_key[0], positions).astype(jnp.bfloat16)
    turned = rotate(queries[0, :, :, NOPE:], positions[:, None])
    query_rot = jnp.concatenate(
        [queries[0, :, :, :NOPE].astype(jnp.float32), turned], axis=-1
    ).astype(jnp.bfloat16)
    query_heads = lax.all_to_all(query_rot[None], "sp", split_axis=2, concat_axis=1, tiled=True)
    every_latent, every_key = (
        lax.all_gather(latent_n[None], "sp", axis=1, tiled=True),
        lax.all_gather(key_rot[None], "sp", axis=1, tiled=True),
    )
    whole_latent = every_latent[0]
    kv_heads = jnp.dot(
        whole_latent, gather_directly(kv_weight, "dp", 0), preferred_element_type=jnp.float32
    ).astype(jnp.bfloat16)
    kv_heads = kv_heads.reshape(whole_latent.shape[0], kv_weight.shape[1] // (NOPE + VD), NOPE + VD)
    attended = attend(query_heads[0], kv_heads, every_key[0])
    returned = lax.all_to_all(attended[None], "sp", split_axis=1, concat_axis=2, tiled=True)
    flat_rows = returned.reshape(tok_rows, returned.shape[2] * returned.shape[3])
    mixed = jnp.dot(
        flat_rows,
        lax.all_gather(out_weight, "dp", axis=1, tiled=True),
        preferred_element_type=jnp.float32,
    ).astype(jnp.bfloat16)
    return mixed[None]


def solution(mesh):
    return jax.shard_map(
        body,
        mesh=mesh,
        in_specs=(
            P(("grp", "dp"), "sp", None, None),
            P(("grp", "dp"), "sp", None),
            P(("grp", "dp"), "sp", None),
            P(),
            P("dp", "sp"),
            P(None, "dp"),
        ),
        out_specs=P(("grp", "dp"), "sp", None),
        check_vma=False,
    )
```

profile of v0, /device:TPU:84, one launch (start us, length us, event | category | flops | bytes accessed | tf_op | source)
XLA Modules:
  0.0 228.3 jit_solution(14194798245144524070)
XLA Ops:
  6.6 1.0 fusion.19
  7.6 1.7 fusion.21
  9.4 0.7 all-gather.5.cloned.1.call-update
  10.1 1.1 slice.32
  11.3 0.9 fusion.29
  12.1 1.0 slice_bitcast_fusion
  13.3 91.7 %all_to_all.35 = bf16[1,128,16,192]{1,3,0,2:T(8,128)(2,1)S(1)} all-to-all(bf16[1,128,16,192]{1,3,0,2:T(8,128)(2,1)S(1)} %pad_maximum_fusion), channel_id=1, replica_groups=mesh['grp'=2,'sp'=16,'dp'=16] {'sp'}, dimensions={2} | all-to-all | bytes 1572864 | tf_op jit(solution)/shard_map/all_to_all | solution.py:87
  104.9 0.7 broadcast_in_dim.13
  105.7 7.8 %all-to-all-start.1 = ((bf16[16,32,256]{2,1,0:T(8,128)(2,1)}), bf16[16,32,256]{2,1,0:T(8,128)(2,1)S(1)}, u32[]{:S(2)}, u32[]{:S(2)}) async-start(bf16[16,32,256]{2,1,0:T(8,128)(2,1)} %broadcast_in_dim.13), calls=%async_computation.1 | async-start | bytes 524288 | tf_op jit(solution)/shard_map/all_to_all | solution.py:12
  113.5 32.2 %all_gather.10 = bf16[1,2048,64]{1,2,0:T(8,128)(2,1)S(1)} all-gather(bf16[1,128,64]{1,2,0:T(8,128)(2,1)S(1)} %pad_maximum_fusion.2), channel_id=1, replica_groups=mesh['grp'=2,'sp'=16,'dp'=16] {'sp'}, dimensions={1}, use_global_device_ids=true | all-gather | bytes 278528 | tf_op jit(solution)/shard_map/all_gather | solution.py:90
  146.7 2.3 %fusion.12 = bf16[2048,1,256]{0,2,1:T(8,128)(2,1)S(1)} fusion(bf16[512,256]{1,0:T(8,128)(2,1)S(1)} %bitcast.82, bf16[1,2048,512]{2,1,0:T(8,128)(2,1)} %all-gather.3.cloned.1.call-done), kind=kOutput, calls=%fused_computation.17 | convolution fusion | flops 537395200 | bytes 3407872 | tf_op jit(solution)/shard_map/dot_general | solution.py:93
  149.1 1.0 copy.27
  150.2 16.9 %while.11 = (s32[]{:T(128)}, bf16[4,512,1,128]{3,1,2,0:T(8,128)(2,1)S(1)}, s32[4]{0:T(128)S(1)}, bf16[4,512,1,192]{1,3,2,0:T(8,128)(2,1)S(1)}, bf16[2048,1,192]{...) while((s32[]{:T(128)}, ...), condition=%wide.region_4.5_spmd.clone, body=%wide.region_1.4_spmd.clone.sunk | while | flops 680590848 | bytes 16332949 | solution.py:69
  150.4 0.6 dynamic_slice.19
  151.5 1.0 fusion.40
  152.5 0.7 fusion.41
  153.7 0.9 fusion.42
  154.6 0.6 dynamic_slice.19
  155.8 1.0 fusion.40
  156.8 0.7 fusion.41
  157.8 0.9 fusion.42
  158.8 0.6 dynamic_slice.19
  159.9 1.0 fusion.40
  160.9 0.7 fusion.41
  162.0 0.9 fusion.42
  164.1 1.0 fusion.40
  165.1 0.7 fusion.41
  166.1 0.9 fusion.42
  167.1 8.1 %copy.32 = bf16[1,2048,1,128]{3,2,0,1:T(2,128)(2,1)S(1)} copy(bf16[1,2048,1,128]{3,1,2,0:T(8,128)(2,1)S(1)} %bitcast.84) | data formatting | bytes 1048576 | tf_op jit(solution)/shard_map/broadcast_in_dim;reshape | solution.py:98
  175.7 11.5 %reduce.5 = bf16[2048,128]{1,0:T(8,128)(2,1)S(1)} reduce(bf16[2048,1,1,128]{3,2,1,0:T(2,128)(2,1)S(1)} %bitcast.78, bf16[]{:T(256)} %broadcast.105), dimensions={1,2}, to_apply=%bitcast.65.reduce_sub_computation | reduce | bytes 1048578
  187.4 27.7 %all_to_all.36 = bf16[16,2,8192]{2,1,0:T(2,128)(2,1)S(1)} all-to-all(bf16[16,2,8192]{2,1,0:T(2,128)(2,1)S(1)} %reshape.234), channel_id=1, replica_groups=mesh['grp'=2,'sp'=16,'dp'=16] {'sp'}, dimensions={0} | all-to-all | bytes 1048576 | tf_op jit(solution)/shard_map/all_to_all | solution.py:98
  216.0 5.5 %fusion.13 = bf16[1,128,2048]{2,1,0:T(8,128)(2,1)} fusion(bf16[128,2048]{0,1:T(8,128)(2,1)S(1)} %bitcast.76, bf16[2048,2048]{1,0:T(8,128)(2,1)} %all-gather.5.cloned.1.call-done), kind=kOutput, calls=%fused_computation.19 | convolution fusion | flops 1074003968 | bytes 9437184 | tf_op jit(solution)/shard_map/dot_general | solution.py:100
  (39 shorter events, 5.0 us)
Async XLA Ops:
  6.5 98.4 %copy-start.1 = (bf16[32,256]{1,0:T(8,128)(2,1)S(1)}, bf16[32,256]{1,0:T(8,128)(2,1)}, u32[]{:S(2)}) copy-start(bf16[32,256]{1,0:T(8,128)(2,1)} %param.12) | copy-start | bytes 49156
  6.5 140.1 %all-gather.3.cloned.1.call-start = ((), (), s32[]{:S(2)}) async-start(), calls=%async_computation.3 | async-start | bytes 2228224 | tf_op jit(solution)/shard_map/all_gather | solution.py:89
  9.3 206.7 %all-gather.5.cloned.1.call-start = ((), (), s32[]{:S(2)}) async-start(), calls=%async_computation.4 | async-start | bytes 8912896 | tf_op jit(solution)/shard_map/all_gather | solution.py:102
  105.7 41.0 %all-to-all-start.1 = ((bf16[16,32,256]{2,1,0:T(8,128)(2,1)}), bf16[16,32,256]{2,1,0:T(8,128)(2,1)S(1)}, u32[]{:S(2)}, u32[]{:S(2)}) async-start(bf16[16,32,256]{2,1,0:T(8,128)(2,1)} %broadcast_in_dim.13), calls=%async_computation.1 | async-start | bytes 524288 | tf_op jit(solution)/shard_map/all_to_all | solution.py:12
  152.5 1.2 copy-start
  156.8 1.0 copy-start
  160.9 1.1 copy-start
  165.1 1.0 copy-start
Sparse Core Ops, SparseCore 0:
  9.4 127.1 all-gather.2
  138.7 67.0 all-gather.4
where the time goes:
time: 229 us; the launch traced here: 228 us
  blocking collectives  152 us (66%)
  local copies, waits for them, and re-layouts  18.1 us (8%)
  other arithmetic  18.1 us (8%)
  matrix products  15.7 us (7%)
  between operations  13.6 us (6%)
  starting transfers between devices  7.86 us (3%)
  loops' own time  2.5 us (1%)
    all_to_all x1, blocking collectives, body(): lax.all_to_all(query_rot[None], 'sp', split_axis=2, concat_axis=1, tiled=...  91.7 us
    all_gather x1, blocking collectives, body(): lax.all_gather(key_rot[None], 'sp', axis=1, tiled=True)  32.2 us
    all_to_all x1, blocking collectives, body(): lax.all_to_all(attended[None], 'sp', split_axis=1, concat_axis=2, tiled=T...  27.7 us
    unnamed x1, other arithmetic  11.5 us
    another operation x1, local copies, waits for them, and re-layouts, body(): attended[None]  8.14 us
    all_to_all x1, starting transfers between devices, sent_to_all(): lax.all_to_all(jnp.broadcast_to(value[None], (length, *value.shape)), axi...  7.79 us
    dot_general x1, matrix products, body(): jnp.dot(flat_rows, lax.all_gather(out_weight, 'dp', axis=1, tiled=True),...  5.46 us
  transfers between devices with their start and end apart: 3, of which 0 were waited for; matrix products, arithmetic and copies ran while one was open for 19% of the time, Pallas kernels for 0%

commit v1 on v0

--- a/solution.py
+++ b/solution.py
@@ -87,7 +87,9 @@
     query_heads = lax.all_to_all(query_rot[None], "sp", split_axis=2, concat_axis=1, tiled=True)
     every_latent, every_key = (
         lax.all_gather(latent_n[None], "sp", axis=1, tiled=True),
-        lax.all_gather(key_rot[None], "sp", axis=1, tiled=True),
+        jnp.concatenate(
+            lax.all_to_all(jnp.stack([key_rot[None]] * lax.axis_size("sp")), "sp", 0, 0), axis=1
+        ),
     )
     whole_latent = every_latent[0]
     kv_heads = jnp.dot(

time: 229 us -> 238 us (1.039)
  the two profiles are of different devices: /device:TPU:84 before, /device:TPU:80 now
where the time goes in v1:
time: 238 us
  blocking collectives  88.8 us (37%)
  starting transfers between devices  53.1 us (22%)
  waiting for transfers between devices  28.2 us (12%)
  other arithmetic  18.4 us (8%)
  local copies, waits for them, and re-layouts  17.1 us (7%)
  matrix products  15.7 us (7%)
  between operations  13.6 us (6%)
  loops' own time  2.7 us (1%)
    all_to_all x1, blocking collectives, body(): lax.all_to_all(query_rot[None], 'sp', split_axis=2, concat_axis=1, tiled=...  52.5 us
    all_to_all x1, starting transfers between devices, body(): lax.all_to_all(jnp.stack([key_rot[None]] * lax.axis_size('sp')), 'sp', 0, 0)  43.7 us
    all_to_all x1, blocking collectives, body(): lax.all_to_all(attended[None], 'sp', split_axis=1, concat_axis=2, tiled=T...  36.4 us
    all_to_all x1, waiting for transfers between devices, body(): lax.all_to_all(jnp.stack([key_rot[None]] * lax.axis_size('sp')), 'sp', 0, 0)  17.7 us
    unnamed x1, other arithmetic  11.7 us
    all_to_all x1, waiting for transfers between devices, sent_to_all(): lax.all_to_all(jnp.broadcast_to(value[None], (length, *value.shape)), axi...  9.65 us
    all_to_all x1, starting transfers between devices, sent_to_all(): lax.all_to_all(jnp.broadcast_to(value[None], (length, *value.shape)), axi...  9.4 us
    another operation x1, local copies, waits for them, and re-layouts, body(): attended[None]  8.14 us
  transfers between devices with their start and end apart: 4, of which 2 were waited for; matrix products, arithmetic and copies ran while one was open for 18% of the time, Pallas kernels for 0%

profile of v1, /device:TPU:80, one launch (start us, length us, event | category | flops | bytes accessed | tf_op | source)
XLA Modules:
  0.0 237.7 jit_solution(11750779639200035465)
XLA Ops:
  6.6 1.0 fusion.19
  7.6 1.7 fusion.21
  9.4 0.7 all-gather.5.cloned.1.call-update
  10.2 0.9 fusion.25
  11.0 0.8 stack.3
  11.8 43.7 %all-to-all-start.2 = ((bf16[16,1,128,64]{2,3,1,0:T(8,128)(2,1)}), bf16[16,1,128,64]{2,3,1,0:T(8,128)(2,1)S(1)}, u32[]{:S(2)}, u32[]{:S(2)}) async-start(bf16[16,1,128,64]{2,3,1,0:T(8,128)(2,1)} %stack.3), calls=%async_computation.2 | async-start | bytes 524288 | tf_op jit(solution)/shard_map/all_to_all | solution.py:91
  55.5 1.1 slice.32
  56.6 1.0 slice_bitcast_fusion
  57.7 17.7 %all-to-all-done.2 = bf16[16,1,128,64]{2,3,1,0:T(8,128)(2,1)S(1)} async-done(((bf16[16,1,128,64]{2,3,1,0:T(8,128)(2,1)}), bf16[16,1,128,64]{2,3,1,0:T(8,128)(2,1)S(1)}, u32[]{:S(2)}, u32[]{:S(2)}) %all-to-all-start.2) | async-done | bytes 262176 | tf_op jit(solution)/shard_map/all_to_all | solution.py:91
  75.4 52.5 %all_to_all.40 = bf16[1,128,16,192]{1,3,0,2:T(8,128)(2,1)S(1)} all-to-all(bf16[1,128,16,192]{1,3,0,2:T(8,128)(2,1)S(1)} %pad_maximum_fusion), channel_id=1, replica_groups=mesh['grp'=2,'sp'=16,'dp'=16] {'sp'}, dimensions={2} | all-to-all | bytes 1572864 | tf_op jit(solution)/shard_map/all_to_all | solution.py:87
  127.9 0.7 broadcast_in_dim.13
  128.6 9.4 %all-to-all-start.1 = ((bf16[16,32,256]{2,1,0:T(8,128)(2,1)}), bf16[16,32,256]{2,1,0:T(8,128)(2,1)S(1)}, u32[]{:S(2)}, u32[]{:S(2)}) async-start(bf16[16,32,256]{2,1,0:T(8,128)(2,1)} %broadcast_in_dim.13), calls=%async_computation.1 | async-start | bytes 524288 | tf_op jit(solution)/shard_map/all_to_all | solution.py:12
  139.3 9.7 %all-to-all-done.1 = bf16[16,32,256]{2,1,0:T(8,128)(2,1)S(1)} async-done(((bf16[16,32,256]{2,1,0:T(8,128)(2,1)}), bf16[16,32,256]{2,1,0:T(8,128)(2,1)S(1)}, u32[]{:S(2)}, u32[]{:S(2)}) %all-to-all-start.1) | async-done | bytes 262176 | tf_op jit(solution)/shard_map/all_to_all | solution.py:12
  149.0 2.3 fusion.12
  151.8 15.8 %while.11 = (s32[]{:T(128)}, bf16[4,512,1,128]{3,1,2,0:T(8,128)(2,1)S(1)}, s32[4]{0:T(128)S(1)}, bf16[4,512,1,192]{1,3,2,0:T(8,128)(2,1)S(1)}, bf16[2048,1,192]{...) while((s32[]{:T(128)}, ...), condition=%wide.region_4.5_spmd.clone, body=%wide.region_1.4_spmd.clone.sunk | while | flops 680590848 | bytes 14235769 | solution.py:69
  151.8 0.6 dynamic_slice.19
  153.0 1.0 fusion.38
  154.1 0.7 fusion.39
  154.8 0.9 fusion.40
  157.0 1.0 fusion.38
  158.0 0.7 fusion.39
  158.7 0.9 fusion.40
  160.9 1.0 fusion.38
  162.0 0.7 fusion.39
  162.7 0.9 fusion.40
  164.9 1.0 fusion.38
  165.9 0.7 fusion.39
  166.6 0.9 fusion.40
  167.6 8.1 %copy.34 = bf16[1,2048,1,128]{3,2,0,1:T(2,128)(2,1)S(1)} copy(bf16[1,2048,1,128]{3,1,2,0:T(8,128)(2,1)S(1)} %bitcast.82) | data formatting | bytes 1048576 | tf_op jit(solution)/shard_map/broadcast_in_dim;reshape | solution.py:100
  176.2 11.7 %reduce.5 = bf16[2048,128]{1,0:T(8,128)(2,1)S(1)} reduce(bf16[2048,1,1,128]{3,2,1,0:T(2,128)(2,1)S(1)} %bitcast.77, bf16[]{:T(256)} %broadcast.107), dimensions={1,2}, to_apply=%bitcast.64.reduce_sub_computation | reduce | bytes 1048578
  188.1 36.4 %all_to_all.41 = bf16[16,2,8192]{2,1,0:T(2,128)(2,1)S(1)} all-to-all(bf16[16,2,8192]{2,1,0:T(2,128)(2,1)S(1)} %reshape.224), channel_id=1, replica_groups=mesh['grp'=2,'sp'=16,'dp'=16] {'sp'}, dimensions={0} | all-to-all | bytes 1048576 | tf_op jit(solution)/shard_map/all_to_all | solution.py:100
  225.4 5.5 %fusion.13 = bf16[1,128,2048]{2,1,0:T(8,128)(2,1)} fusion(bf16[128,2048]{0,1:T(8,128)(2,1)S(1)} %bitcast.75, bf16[2048,2048]{1,0:T(8,128)(2,1)} %all-gather.5.cloned.1.call-done), kind=kOutput, calls=%fused_computation.19 | convolution fusion | flops 1074003968 | bytes 9437184 | tf_op jit(solution)/shard_map/dot_general | solution.py:102
  (35 shorter events, 5.3 us)
Async XLA Ops:
  6.5 121.4 %copy-start = (bf16[32,256]{1,0:T(8,128)(2,1)S(1)}, bf16[32,256]{1,0:T(8,128)(2,1)}, u32[]{:S(2)}) copy-start(bf16[32,256]{1,0:T(8,128)(2,1)} %param.12) | copy-start | bytes 49156
  6.5 142.4 %all-gather.3.cloned.1.call-start = ((), (), s32[]{:S(2)}) async-start(), calls=%async_computation.4 | async-start | bytes 2228224 | tf_op jit(solution)/shard_map/all_gather | solution.py:89
  9.3 216.1 %all-gather.5.cloned.1.call-start = ((), (), s32[]{:S(2)}) async-start(), calls=%async_computation.5 | async-start | bytes 8912896 | tf_op jit(solution)/shard_map/all_gather | solution.py:104
  11.8 63.6 %all-to-all-start.2 = ((bf16[16,1,128,64]{2,3,1,0:T(8,128)(2,1)}), bf16[16,1,128,64]{2,3,1,0:T(8,128)(2,1)S(1)}, u32[]{:S(2)}, u32[]{:S(2)}) async-start(bf16[16,1,128,64]{2,3,1,0:T(8,128)(2,1)} %stack.3), calls=%async_computation.2 | async-start | bytes 524288 | tf_op jit(solution)/shard_map/all_to_all | solution.py:91
  128.6 20.3 %all-to-all-start.1 = ((bf16[16,32,256]{2,1,0:T(8,128)(2,1)}), bf16[16,32,256]{2,1,0:T(8,128)(2,1)S(1)}, u32[]{:S(2)}, u32[]{:S(2)}) async-start(bf16[16,32,256]{2,1,0:T(8,128)(2,1)} %broadcast_in_dim.13), calls=%async_computation.1 | async-start | bytes 524288 | tf_op jit(solution)/shard_map/all_to_all | solution.py:12
Sparse Core Ops, SparseCore 0:
  9.4 134.2 all-gather.2
  145.8 66.3 all-gather.4
